TPU v7x, 512 devices: a whole 4x4x16 slice. The times are simulated.
512 devices in a mesh: fs: 16 (over y, x), tp: 32 (over z, core).
Axes of the slice: x: 4, y: 4, z: 16, core: 2. Of those that a mesh axis runs over, the one named last changes fastest.
Arguments:
- tokens: bfloat16 [8192, 2048], P('fs', 'tp'), may hold values from -6 to 6
- norm_gain: float32 [2048], P('fs'), may hold values from 0.1 to 1.9
- gate_train: float32 [2048, 8192], P('fs', 'tp'), may hold values from -0.125 to 0.125
- up_train: float32 [2048, 8192], P('fs', 'tp'), may hold values from -0.125 to 0.125
- down_train: float32 [8192, 2048], P('fs', 'tp'), may hold values from -0.0625 to 0.0625
Outputs:
- gate_serve: bfloat16 [2048, 8192], P(None, 'tp')
- up_serve: bfloat16 [2048, 8192], P(None, 'tp')
- down_serve: bfloat16 [8192, 2048], P('tp')
- layer_out: bfloat16 [8192, 2048], P(('fs', 'tp'))
All inputs are finite; a program needn't handle non-finite values.
Results may differ from a plain program's by a relative error of at most 0.024.
Values may be sent and summed in bfloat16 or wider, within the bound.
No kernel may reach another device: no remote copies, remote signals or barrier semaphores. Data moves between devices by JAX's collectives and lax.ppermute only.
A program may use at most 64 MiB of HBM per device.

v0:
```python
import jax
import jax.numpy as jnp
from jax import lax
from jax.sharding import Mesh
from jax.sharding import PartitionSpec as P

D = 2048
TP = ("tp_0", "tp_1")
FS_TP = ("fs", "tp_0", "tp_1")
epsilon = 1e-06


def side_by_side(arrays, axis, dim, along):
    both = jnp.concatenate(arrays, axis=along)
    whole, at, finished = (lax.all_gather(both, axis, axis=dim, tiled=True), 0, [])
    for a in arrays:
        finished.append(lax.slice_in_dim(whole, at, at + a.shape[along], axis=along))
        at += a.shape[along]
    return tuple(finished)


def joined_along(pieces, dim):
    shape = list(pieces.shape[1:])
    shape[dim] *= pieces.shape[0]
    return jnp.moveaxis(pieces, 0, dim).reshape(shape)


def copy_for_each(x, axis):
    copies = jnp.broadcast_to(x, (lax.axis_size(axis), *x.shape))
    return lax.all_to_all(copies, axis, split_axis=0, concat_axis=0, tiled=True)


def collect(x, axis, dim):
    return joined_along(copy_for_each(x, axis), dim)


def sum_in_order(pieces, axes, order):
    shape = [lax.axis_size(a) for a in axes]
    pieces = pieces.reshape(*shape, *pieces.shape[1:])
    pieces = pieces.transpose(*order, *range(len(axes), pieces.ndim))
    pieces = pieces.reshape(-1, *pieces.shape[len(axes) :])
    for k in order:
        pieces = lax.psum_scatter(pieces, axes[k], scatter_dimension=0, tiled=True)
    return pieces[0]


def cut_along(x, dim, count):
    before, after = (x.shape[:dim], x.shape[dim + 1 :])
    return jnp.moveaxis(x.reshape(*before, count, -1, *after), dim, 0)


def sum_by_axis(x, axes, order, dim):
    count = lax.axis_size(axes)
    return sum_in_order(cut_along(x, dim, count), axes, order)


def body(tokens, norm_gain, gate_train, up_train, down_train):
    gate_local = (norm_gain[:, None] * gate_train).astype(jnp.bfloat16)
    up_local = (norm_gain[:, None] * up_train).astype(jnp.bfloat16)
    down_local = down_train.astype(jnp.bfloat16)
    features = lax.all_gather(tokens, TP, axis=1, tiled=True)
    wide = features.astype(jnp.float32)
    squares = jnp.sum(wide * wide, axis=1)
    gate_whole, up_whole = side_by_side((gate_local, up_local), "fs", 0, 1)
    gate_sum = jnp.dot(features, gate_whole, preferred_element_type=jnp.float32)
    up_sum = jnp.dot(features, up_whole, preferred_element_type=jnp.float32)
    down_rows = collect(down_local, "fs", 0)
    down_whole = lax.all_to_all(down_rows, TP, split_axis=0, concat_axis=1, tiled=True)
    scale = lax.rsqrt(squares / D + epsilon)[:, None]
    hidden = (jax.nn.silu(gate_sum * scale) * (up_sum * scale)).astype(jnp.bfloat16)
    mixed = (
        sum_by_axis(
            jnp.dot(hidden, down_whole, preferred_element_type=jnp.float32).astype(jnp.bfloat16),
            TP,
            (1, 0),
            0,
        )
        .astype(jnp.float32)
        .astype(jnp.bfloat16)
    )
    return (gate_whole, up_whole, down_whole, mixed)


def solution(mesh):
    finer = Mesh(mesh.devices.reshape(mesh.shape["fs"], 16, 2), ("fs", "tp_0", "tp_1"))
    placed = (P("fs", TP), P("fs"), P("fs", TP), P("fs", TP), P("fs", TP))
    return jax.shard_map(
        body,
        mesh=finer,
        in_specs=placed,
        out_specs=(P(None, TP), P(None, TP), P(TP, None), P(FS_TP, None)),
        check_vma=False,
    )
```

profile of v0, /device:TPU:2, one launch (start us, length us, event | category | flops | bytes accessed | tf_op | source)
XLA Modules:
  0.0 262.0 jit_solution(8087558812155801704)
XLA Ops:
  7.2 0.0 all-gather.3.cloned.1.call-start
  7.2 1.1 multiply_convert_fusion.1
  8.3 0.7 pad_maximum_fusion
  9.0 0.9 convert_element_type.22
  9.9 1.1 broadcast_in_dim.2
  11.0 9.3 %all-to-all-start = ((bf16[16,512,64]{1,2,0:T(8,128)(2,1)}), bf16[16,512,64]{1,2,0:T(8,128)(2,1)S(1)}, u32[]{:S(2)}, u32[]{:S(2)}) async-start(bf16[16,512,64]{1,2,0:T(8,128)(2,1)} %broadcast_in_dim.2), calls=%async_computation | async-start | bytes 2097152 | tf_op jit(solution)/shard_map/all_to_all | solution.py:30
  20.3 0.7 all-gather.5.cloned.1.call-update
  21.0 13.6 %all-to-all-done = bf16[16,512,64]{1,2,0:T(8,128)(2,1)S(1)} async-done(((bf16[16,512,64]{1,2,0:T(8,128)(2,1)}), bf16[16,512,64]{1,2,0:T(8,128)(2,1)S(1)}, u32[]{:S(2)}, u32[]{:S(2)}) %all-to-all-start) | async-done | bytes 1048608 | tf_op jit(solution)/shard_map/all_to_all | solution.py:30
  34.7 0.6 copy.14
  35.2 0.4 all_to_all.18
  35.6 1.6 copy.15
  37.2 15.0 %all-to-all-start.1 = ((bf16[32,256,64]{1,2,0:T(8,128)(2,1)}), bf16[32,256,64]{1,2,0:T(8,128)(2,1)S(1)}, u32[]{:S(2)}, u32[]{:S(2)}) async-start(bf16[32,256,64]{1,2,0:T(8,128)(2,1)} %copy.15), calls=%async_computation.1 | async-start | bytes 2097152 | tf_op jit(solution)/shard_map/all_to_all | solution.py:68
  52.3 0.0 reduce-scatter.3.cloned.1.call-start
  52.3 23.6 %all-gather.3.cloned.1.call-done = bf16[2048,512]{1,0:T(8,128)(2,1)} async-done(((bf16[128,512]{1,0:T(8,128)(2,1)}), bf16[2048,512]{1,0:T(8,128)(2,1)}) %all-gather.3.cloned.1.call-update) | async-done | bytes 2097168 | tf_op jit(solution)/shard_map/all_gather | solution.py:15
  75.9 3.0 %fusion.12 = (bf16[2048,256]{1,0:T(8,128)(2,1)}, bf16[2048,256]{1,0:T(8,128)(2,1)}) fusion(bf16[2048,512]{1,0:T(8,128)(2,1)} %all-gather.3.cloned.1.call-done), kind=kLoop, calls=%fused_computation.20 | loop fusion | bytes 4194304 | tf_op jit(solution)/shard_map/slice | solution.py:17
  78.9 71.5 %all-gather.5.cloned.1.call-done = bf16[512,2048]{0,1:T(8,128)(2,1)} async-done(((bf16[512,64]{0,1:T(8,128)(2,1)}), bf16[512,2048]{0,1:T(8,128)(2,1)}) %all-gather.5.cloned.1.call-update) | async-done | bytes 2097168 | tf_op jit(solution)/shard_map/all_gather | solution.py:61
  150.4 2.2 multiply_reduce_fusion
  152.7 2.8 %fusion.2 = f32[512,256]{0,1:T(8,128)} fusion(bf16[2048,256]{1,0:T(8,128)(2,1)} %get-tuple-element.13, bf16[512,2048]{0,1:T(8,128)(2,1)S(1)} %copy-done, f32[512]{0:T(512)S(1)} %add_rsqrt_fusion), kind=kOutput, calls=%fused_computation.6 | convolution fusion | flops 537001984 | bytes 3672064 | tf_op jit(solution)/shard_map/dot_general | solution.py:65
  155.5 4.2 %convolution_convert_fusion = bf16[512,2048]{1,0:T(8,128)(2,1)} fusion(bf16[256,2048]{0,1:T(8,128)(2,1)S(1)} %bitcast.26, bf16[2048,256]{1,0:T(8,128)(2,1)} %get-tuple-element.12, bf16[512,2048]{0,1:T(8,128)(2,1)S(1)} %copy-done, f32[512,256]{0,1:T(8,128)} %fusion.2, f32[512]{0:T(512)S(1)} %add_rsqrt_fusion), kind=kOutput, calls=%fused_computation.1 | convolution fusion | flops 1075707904 | bytes 6817792 | tf_op jit(solution)/shard_map/dot_general | solution.py:73
  159.7 3.2 %copy.16 = bf16[2,16,16,2048]{3,2,1,0:T(8,128)(2,1)} copy(bf16[2,16,16,2048]{3,2,0,1:T(8,128)(2,1)} %bitcast.28) | data formatting | bytes 4194304 | tf_op jit(solution)/shard_map/transpose | solution.py:40
  162.8 0.0 reduce-scatter.5.cloned.1.call-start
  162.9 16.7 %reduce-scatter.3.cloned.1.call-done = bf16[16,16,2048]{2,1,0:T(8,128)(2,1)} async-done(((bf16[32,16,2048]{2,1,0:T(8,128)(2,1)}), bf16[16,16,2048]{2,1,0:T(8,128)(2,1)}) %reduce-scatter.3.cloned.1.call-update) | async-done | bytes 1048592 | tf_op jit(solution)/shard_map/reduce_scatter | solution.py:43
  179.6 1.4 copy.17
  181.0 74.5 %reduce-scatter.5.cloned.1.call-done = bf16[1,16,2048]{2,1,0:T(8,128)(2,1)} async-done(((bf16[16,16,2048]{2,1,0:T(8,128)(2,1)}), bf16[1,16,2048]{2,1,0:T(8,128)(2,1)}) %reduce-scatter.5.cloned.1.call-update) | async-done | bytes 65552 | tf_op jit(solution)/shard_map/reduce_scatter | solution.py:43
  (8 shorter events, 0.1 us)
Async XLA Ops:
  7.2 68.8 %all-gather.3.cloned.1.call-start = ((), (), s32[]{:S(2)}) async-start(), calls=%async_computation.4 | async-start | bytes 2228224 | tf_op jit(solution)/shard_map/all_gather | solution.py:15
  11.0 23.7 %all-to-all-start = ((bf16[16,512,64]{1,2,0:T(8,128)(2,1)}), bf16[16,512,64]{1,2,0:T(8,128)(2,1)S(1)}, u32[]{:S(2)}, u32[]{:S(2)}) async-start(bf16[16,512,64]{1,2,0:T(8,128)(2,1)} %broadcast_in_dim.2), calls=%async_computation | async-start | bytes 2097152 | tf_op jit(solution)/shard_map/all_to_all | solution.py:30
  20.3 130.1 %all-gather.5.cloned.1.call-start = ((), (), s32[]{:S(2)}) async-start(), calls=%async_computation.5 | async-start | bytes 2162688 | tf_op jit(solution)/shard_map/all_gather | solution.py:61
  37.2 118.3 %all-to-all-start.1 = ((bf16[32,256,64]{1,2,0:T(8,128)(2,1)}), bf16[32,256,64]{1,2,0:T(8,128)(2,1)S(1)}, u32[]{:S(2)}, u32[]{:S(2)}) async-start(bf16[32,256,64]{1,2,0:T(8,128)(2,1)} %copy.15), calls=%async_computation.1 | async-start | bytes 2097152 | tf_op jit(solution)/shard_map/all_to_all | solution.py:68
  52.3 127.3 %reduce-scatter.3.cloned.1.call-start = ((), (), s32[]{:S(2)}) async-start(), calls=%async_computation.6 | async-start | bytes 3145728 | tf_op jit(solution)/shard_map/reduce_scatter | solution.py:43
  150.4 2.3 copy-start
  162.8 92.6 %reduce-scatter.5.cloned.1.call-start = ((), (), s32[]{:S(2)}) async-start(), calls=%async_computation.7 | async-start | bytes 1114112 | tf_op jit(solution)/shard_map/reduce_scatter | solution.py:43
Sparse Core Ops, SparseCore 0:
  11.6 64.3 all-gather.2
  78.1 72.3 all-gather.4
  163.0 16.5 reduce-scatter.2
  182.8 72.6 reduce-scatter.4
where the time goes:
time: 262 us
  waiting for transfers between devices  201 us (77%)
  starting transfers between devices  24.5 us (9%)
  between operations  13.8 us (5%)
  local copies, waits for them, and re-layouts  11.2 us (4%)
  matrix products  6.97 us (3%)
  other arithmetic  4.91 us (2%)
    reduce_scatter x2, waiting for transfers between devices, sum_in_order(): pieces = lax.psum_scatter(pieces, axes[k], scatter_dimension=0, tiled=True)  91.2 us
    all_gather x1, waiting for transfers between devices, body(): features = lax.all_gather(tokens, TP, axis=1, tiled=True)  71.5 us
    all_gather x1, waiting for transfers between devices, side_by_side(): lax.all_gather(both, axis, axis=dim, tiled=True)  23.6 us
    all_to_all x1, starting transfers between devices, body(): lax.all_to_all(down_rows, TP, split_axis=0, concat_axis=1, tiled=True)  15 us
    all_to_all x1, waiting for transfers between devices, copy_for_each(): return lax.all_to_all(copies, axis, split_axis=0, concat_axis=0, tiled=True)  13.6 us
    all_to_all x1, starting transfers between devices, copy_for_each(): return lax.all_to_all(copies, axis, split_axis=0, concat_axis=0, tiled=True)  9.32 us
  transfers between devices with their start and end apart: 6, of which 5 were waited for; matrix products, arithmetic and copies ran while one was open for 5% of the time, Pallas kernels for 0%

commit v1 on v0

--- a/solution.py
+++ b/solution.py
@@ -65,7 +65,9 @@
     gate_sum = jnp.dot(features, gate_whole, preferred_element_type=jnp.float32)
     up_sum = jnp.dot(features, up_whole, preferred_element_type=jnp.float32)
     down_rows = collect(down_local, "fs", 0)
-    down_whole = lax.all_to_all(down_rows, TP, split_axis=0, concat_axis=1, tiled=True)
+    cells = jnp.split(down_rows, lax.axis_size(TP), axis=0)
+    received = lax.all_to_all(jnp.stack(cells), TP, 0, 0)
+    down_whole = jnp.concatenate(received, axis=1)
     scale = lax.rsqrt(squares / D + epsilon)[:, None]
     hidden = (jax.nn.silu(gate_sum * scale) * (up_sum * scale)).astype(jnp.bfloat16)
     mixed = (

time: 262 us -> 269 us (1.027)
  local copies, waits for them, and re-layouts: 11.2 us -> 28.6 us
  waiting for transfers between devices: 201 us -> 190 us
    unnamed x3 -> x34, local copies, waits for them, and re-layouts: 1.43 us -> 20.6 us
    all_gather x1, waiting for transfers between devices: 23.6 us -> 6.24 us  [side_by_side(): lax.all_gather(both, axis, axis=dim, tiled=True)]
    all_gather x1, waiting for transfers between devices: 71.5 us -> 77.7 us  [body(): features = lax.all_gather(tokens, TP, axis=1, tiled=True)]
  transfers between devices with their start and end apart: 6 -> 6, of which waited for: 5 -> 5; matrix products, arithmetic and copies ran while one was open for 5% -> 12% of each run, Pallas kernels for 0% -> 0%
where the time goes in v1:
time: 269 us; the launch traced here: 268 us
  waiting for transfers between devices  190 us (71%)
  local copies, waits for them, and re-layouts  28.6 us (11%)
  starting transfers between devices  24.5 us (9%)
  between operations  13.8 us (5%)
  matrix products  6.96 us (3%)
  other arithmetic  4.91 us (2%)
    reduce_scatter x2, waiting for transfers between devices, sum_in_order(): pieces = lax.psum_scatter(pieces, axes[k], scatter_dimension=0, tiled=True)  91.5 us
    all_gather x1, waiting for transfers between devices, body(): features = lax.all_gather(tokens, TP, axis=1, tiled=True)  77.7 us
    unnamed x34, local copies, waits for them, and re-layouts  20.6 us
    all_to_all x1, starting transfers between devices, body(): received = lax.all_to_all(jnp.stack(cells), TP, 0, 0)  15 us
    all_to_all x1, waiting for transfers between devices, copy_for_each(): return lax.all_to_all(copies, axis, split_axis=0, concat_axis=0, tiled=True)  13.6 us
    all_to_all x1, starting transfers between devices, copy_for_each(): return lax.all_to_all(copies, axis, split_axis=0, concat_axis=0, tiled=True)  9.32 us
    all_gather x1, waiting for transfers between devices, side_by_side(): lax.all_gather(both, axis, axis=dim, tiled=True)  6.24 us
  transfers between devices with their start and end apart: 6, of which 5 were waited for; matrix products, arithmetic and copies ran while one was open for 12% of the time, Pallas kernels for 0%

profile of v1, /device:TPU:2, one launch (start us, length us, event | category | flops | bytes accessed | tf_op | source)
XLA Modules:
  0.0 268.5 jit_solution(5697342496282210753)
XLA Ops:
  7.2 1.1 multiply_convert_fusion.1
  8.3 0.7 pad_maximum_fusion
  9.0 0.9 convert_element_type.22
  9.9 1.1 broadcast_in_dim.2
  11.0 9.3 %all-to-all-start = ((bf16[16,512,64]{1,2,0:T(8,128)(2,1)}), bf16[16,512,64]{1,2,0:T(8,128)(2,1)S(1)}, u32[]{:S(2)}, u32[]{:S(2)}) async-start(bf16[16,512,64]{1,2,0:T(8,128)(2,1)} %broadcast_in_dim.2), calls=%async_computation | async-start | bytes 2097152 | tf_op jit(solution)/shard_map/all_to_all | solution.py:30
  20.3 0.7 all-gather.5.cloned.1.call-update
  21.0 13.6 %all-to-all-done = bf16[16,512,64]{1,2,0:T(8,128)(2,1)S(1)} async-done(((bf16[16,512,64]{1,2,0:T(8,128)(2,1)}), bf16[16,512,64]{1,2,0:T(8,128)(2,1)S(1)}, u32[]{:S(2)}, u32[]{:S(2)}) %all-to-all-start) | async-done | bytes 1048608 | tf_op jit(solution)/shard_map/all_to_all | solution.py:30
  34.8 0.6 constant_dynamic-update-slice_fusion.31
  35.4 0.6 constant_dynamic-update-slice_fusion.30
  37.2 0.6 constant_dynamic-update-slice_fusion.27
  39.1 0.6 constant_dynamic-update-slice_fusion.24
  41.0 0.6 constant_dynamic-update-slice_fusion.21
  42.8 0.6 constant_dynamic-update-slice_fusion.18
  54.6 15.0 %all-to-all-start.1 = ((bf16[32,256,64]{1,2,0:T(8,128)(2,1)}), bf16[32,256,64]{1,2,0:T(8,128)(2,1)S(1)}, u32[]{:S(2)}, u32[]{:S(2)}) async-start(bf16[32,256,64]{1,2,0:T(8,128)(2,1)} %constant_dynamic-update-slice_fusion), calls=%async_computation.1 | async-start | bytes 2097152 | tf_op jit(solution)/shard_map/all_to_all | solution.py:69
  69.7 6.2 %all-gather.3.cloned.1.call-done = bf16[2048,512]{1,0:T(8,128)(2,1)} async-done(((bf16[128,512]{1,0:T(8,128)(2,1)}), bf16[2048,512]{1,0:T(8,128)(2,1)}) %all-gather.3.cloned.1.call-update) | async-done | bytes 2097168 | tf_op jit(solution)/shard_map/all_gather | solution.py:15
  75.9 3.0 %fusion.12 = (bf16[2048,256]{1,0:T(8,128)(2,1)}, bf16[2048,256]{1,0:T(8,128)(2,1)}) fusion(bf16[2048,512]{1,0:T(8,128)(2,1)} %all-gather.3.cloned.1.call-done), kind=kLoop, calls=%fused_computation.84 | loop fusion | bytes 4194304 | tf_op jit(solution)/shard_map/slice | solution.py:17
  78.9 77.7 %all-gather.5.cloned.1.call-done = bf16[512,2048]{0,1:T(8,128)(2,1)} async-done(((bf16[512,64]{0,1:T(8,128)(2,1)}), bf16[512,2048]{0,1:T(8,128)(2,1)}) %all-gather.5.cloned.1.call-update) | async-done | bytes 2097168 | tf_op jit(solution)/shard_map/all_gather | solution.py:61
  156.6 2.2 multiply_reduce_fusion
  158.9 2.8 %fusion.2 = f32[512,256]{0,1:T(8,128)} fusion(bf16[2048,256]{1,0:T(8,128)(2,1)} %get-tuple-element.13, bf16[512,2048]{0,1:T(8,128)(2,1)S(1)} %copy-done, f32[512]{0:T(512)S(1)} %add_rsqrt_fusion), kind=kOutput, calls=%fused_computation.6 | convolution fusion | flops 537001984 | bytes 3672064 | tf_op jit(solution)/shard_map/dot_general | solution.py:65
  161.6 4.2 %convolution_convert_fusion = bf16[512,2048]{1,0:T(8,128)(2,1)} fusion(bf16[256,2048]{0,1:T(8,128)(2,1)S(1)} %bitcast.186, bf16[2048,256]{1,0:T(8,128)(2,1)} %get-tuple-element.12, bf16[512,2048]{0,1:T(8,128)(2,1)S(1)} %copy-done, f32[512,256]{0,1:T(8,128)} %fusion.2, f32[512]{0:T(512)S(1)} %add_rsqrt_fusion), kind=kOutput, calls=%fused_computation.1 | convolution fusion | flops 1075707904 | bytes 6817792 | tf_op jit(solution)/shard_map/dot_general | solution.py:75
  165.8 3.2 %copy.45 = bf16[2,16,16,2048]{3,2,1,0:T(8,128)(2,1)} copy(bf16[2,16,16,2048]{3,2,0,1:T(8,128)(2,1)} %bitcast.189) | data formatting | bytes 4194304 | tf_op jit(solution)/shard_map/transpose | solution.py:40
  169.1 16.9 %reduce-scatter.3.cloned.1.call-done = bf16[16,16,2048]{2,1,0:T(8,128)(2,1)} async-done(((bf16[32,16,2048]{2,1,0:T(8,128)(2,1)}), bf16[16,16,2048]{2,1,0:T(8,128)(2,1)}) %reduce-scatter.3.cloned.1.call-update) | async-done | bytes 1048592 | tf_op jit(solution)/shard_map/reduce_scatter | solution.py:43
  186.0 1.4 copy.46
  187.4 74.5 %reduce-scatter.5.cloned.1.call-done = bf16[1,16,2048]{2,1,0:T(8,128)(2,1)} async-done(((bf16[16,16,2048]{2,1,0:T(8,128)(2,1)}), bf16[1,16,2048]{2,1,0:T(8,128)(2,1)}) %reduce-scatter.5.cloned.1.call-update) | async-done | bytes 65552 | tf_op jit(solution)/shard_map/reduce_scatter | solution.py:43
  (38 shorter events, 16.4 us)
Async XLA Ops:
  7.2 68.8 %all-gather.3.cloned.1.call-start = ((), (), s32[]{:S(2)}) async-start(), calls=%async_computation.4 | async-start | bytes 2228224 | tf_op jit(solution)/shard_map/all_gather | solution.py:15
  11.0 23.7 %all-to-all-start = ((bf16[16,512,64]{1,2,0:T(8,128)(2,1)}), bf16[16,512,64]{1,2,0:T(8,128)(2,1)S(1)}, u32[]{:S(2)}, u32[]{:S(2)}) async-start(bf16[16,512,64]{1,2,0:T(8,128)(2,1)} %broadcast_in_dim.2), calls=%async_computation | async-start | bytes 2097152 | tf_op jit(solution)/shard_map/all_to_all | solution.py:30
  20.3 136.3 %all-gather.5.cloned.1.call-start = ((), (), s32[]{:S(2)}) async-start(), calls=%async_computation.5 | async-start | bytes 2162688 | tf_op jit(solution)/shard_map/all_gather | solution.py:61
  54.6 107.0 %all-to-all-start.1 = ((bf16[32,256,64]{1,2,0:T(8,128)(2,1)}), bf16[32,256,64]{1,2,0:T(8,128)(2,1)S(1)}, u32[]{:S(2)}, u32[]{:S(2)}) async-start(bf16[32,256,64]{1,2,0:T(8,128)(2,1)} %constant_dynamic-update-slice_fusion), calls=%async_computation.1 | async-start | bytes 2097152 | tf_op jit(solution)/shard_map/all_to_all | solution.py:69
  69.6 116.3 %reduce-scatter.3.cloned.1.call-start = ((), (), s32[]{:S(2)}) async-start(), calls=%async_computation.6 | async-start | bytes 3145728 | tf_op jit(solution)/shard_map/reduce_scatter | solution.py:43
  156.6 2.3 copy-start
  169.0 93.0 %reduce-scatter.5.cloned.1.call-start = ((), (), s32[]{:S(2)}) async-start(), calls=%async_computation.7 | async-start | bytes 1114112 | tf_op jit(solution)/shard_map/reduce_scatter | solution.py:43
Sparse Core Ops, SparseCore 0:
  11.6 64.3 all-gather.2
  78.1 78.4 all-gather.4
  169.1 16.8 reduce-scatter.2
  189.2 72.7 reduce-scatter.4
